TPU v7x, 32 devices: a whole 2x2x4 slice. The times are simulated.
32 devices in a mesh: sp: 16 (over z, y, core), tp: 2 (over x).
Axes of the slice: x: 2, y: 2, z: 4, core: 2. Of those that a mesh axis runs over, the one named last changes fastest.
Arguments:
- queries: bfloat16 [8192, 1024], P('sp', 'tp'), may hold values from -160 to 160
- keys: bfloat16 [8192, 256], P('sp', 'tp'), may hold values from -5 to 5
- values: bfloat16 [8192, 256], P('sp', 'tp'), may hold values from -6 to 6
- doc_ids: int32 [8192], P('sp'), may hold values from 0 to 7, never falling along the last dimension, each value on 1 to 2048 neighbouring positions
- sink_logit: float32 [16], P('tp'), may hold values from 1 to 6
- w_out: bfloat16 [1024, 2048], P('tp'), may hold values from -0.1875 to 0.1875
- residual: bfloat16 [8192, 2048], P(('sp', 'tp')), may hold values from -6 to 6
- ffn_gain: float32 [2048], replicated, may hold values from 0.1 to 1.9
- expert_ids: int32 [8192, 8], P(('sp', 'tp')), may hold values from 0 to 15, all different within a row; in each aligned block of 128 rows (0 to 127, 128 to 255, ...) at most 96 rows name the same one
- expert_weight: float32 [8192, 8], P(('sp', 'tp')), may hold values from 0.2 to 2
- exp_gate: bfloat16 [16, 2048, 512], P('sp'), may hold values from -0.125 to 0.125
- exp_up: bfloat16 [16, 2048, 512], P('sp'), may hold values from -0.125 to 0.125
- exp_down: bfloat16 [16, 512, 2048], P('sp'), may hold values from -0.25 to 0.25
- shared_gate: bfloat16 [2048, 512], P(None, 'tp'), may hold values from -0.125 to 0.125
- shared_up: bfloat16 [2048, 512], P(None, 'tp'), may hold values from -0.125 to 0.125
- shared_down: bfloat16 [512, 2048], P('tp'), may hold values from -0.25 to 0.25
Outputs:
- output: bfloat16 [8192, 2048], P(('sp', 'tp'))
Inputs may be any that keep to these rules, and one draw needn't show every extreme that they name: `doc_ids`: never falling along the sequence; every document holds at most 2048 positions, and one holds exactly that many. `expert_ids`: each row names 8 different experts. In each aligned block of 128 rows no expert is named by more than 96 rows, and in some blocks one expert is named by exactly 96 rows.
All inputs are finite; a program needn't handle non-finite values.
Results may differ from a plain program's by a relative error of at most 0.018.
Values may be sent and summed in bfloat16 or wider, within the bound.
A program may use at most 128 MiB of HBM per device.

v0:
```python
import jax
import jax.numpy as jnp
from jax import lax
from jax.sharding import PartitionSpec as P

HD = 64
WINDOW = 128
norm_eps = 1e-06


def extended(cells, sides, width):
    for axis, dim in sides:
        count = lax.axis_size(axis)
        ends = count - 1
        head = lax.slice_in_dim(cells, 0, width, axis=dim)
        tail = lax.slice_in_dim(cells, cells.shape[dim] - width, cells.shape[dim], axis=dim)
        cells = jnp.concatenate(
            [
                lax.ppermute(tail, axis, [(i, (i + 1) % count) for i in range(ends)]),
                cells,
                lax.ppermute(head, axis, [((i + 1) % count, i) for i in range(ends)]),
            ],
            axis=dim,
        )
    return cells


def band_blocks(padded, width):
    span_count = padded.shape[0] // width - 2
    shaped = padded.reshape((span_count + 2, width) + padded.shape[1:])
    return jnp.concatenate(
        [
            shaped[0:span_count:2],
            shaped[1 : span_count + 1 : 2],
            shaped[2 : span_count + 2 : 2],
            shaped[3 : span_count + 3 : 2],
        ],
        axis=1,
    )


def attend(queries, ext_keys, ext_values, ext_marks, own_marks, sink_logit):
    tok_count = queries.shape[0]
    head_count = sink_logit.shape[0]
    key_heads = ext_keys.shape[1] // HD
    group_size = head_count // key_heads
    query_span = 2 * WINDOW
    block_count = tok_count // query_span
    query_blocks = queries.reshape(block_count, query_span, key_heads, group_size, HD)
    key_blocks = band_blocks(ext_keys, WINDOW).reshape(block_count, 4 * WINDOW, key_heads, HD)
    value_blocks = band_blocks(ext_values, WINDOW).reshape(block_count, 4 * WINDOW, key_heads, HD)
    mark_blocks = band_blocks(ext_marks, WINDOW)
    query_marks = own_marks.reshape(block_count, query_span)
    scores = jnp.einsum(
        "nqkgd,nmkd->nkgqm", query_blocks, key_blocks, preferred_element_type=jnp.float32
    ) * HD ** (-0.5)
    offset = (
        jnp.arange(query_span, dtype=jnp.int32)[:, None]
        - jnp.arange(4 * WINDOW, dtype=jnp.int32)[None, :]
        + WINDOW
    )
    allowed = (jnp.abs(offset) <= WINDOW)[None] & (
        mark_blocks[:, None, :] == query_marks[:, :, None]
    )
    scores = jnp.where(allowed[:, None, None], scores, -jnp.inf)
    sink_term = sink_logit.reshape(key_heads, group_size)[None, :, :, None, None]
    row_max = jnp.maximum(jnp.max(scores, axis=-1, keepdims=True), sink_term)
    exp_scores = jnp.exp(scores - row_max)
    attn_probs = (
        exp_scores / (jnp.sum(exp_scores, axis=-1, keepdims=True) + jnp.exp(sink_term - row_max))
    ).astype(jnp.bfloat16)
    result = jnp.einsum(
        "nkgqm,nmkd->nqkgd", attn_probs, value_blocks, preferred_element_type=jnp.float32
    )
    return result.astype(jnp.bfloat16).reshape(tok_count, head_count * HD)


def slot_index(routing, half_rows, slot_cap, expert_count):
    blocks = routing.shape[0] // half_rows
    flat_ids = routing.reshape(blocks, half_rows * routing.shape[1])
    onehot = (
        flat_ids[:, :, None] == jnp.arange(expert_count, dtype=jnp.int32)[None, None, :]
    ).astype(jnp.int32)
    slot_rank = jnp.sum(jnp.cumsum(onehot, axis=1) * onehot, axis=-1) - 1
    slot_place = (
        flat_ids * (blocks * slot_cap)
        + jnp.arange(blocks, dtype=jnp.int32)[:, None] * slot_cap
        + slot_rank
    )
    return slot_place.reshape(-1)


def pack_rows(normed, slot_place, expert_count, per_expert):
    assign_count = slot_place.shape[0]
    top_count = assign_count // normed.shape[0]
    source = (
        jnp.full((expert_count * per_expert,), normed.shape[0], jnp.int32)
        .at[slot_place]
        .set(jnp.arange(assign_count, dtype=jnp.int32) // top_count)
    )
    packed = jnp.take(normed, source, axis=0, mode="fill", fill_value=0)
    return packed.reshape(expert_count, per_expert, normed.shape[1])


def run_expert(arrived, gate_w, up_w, down_w):
    flat_rows = arrived.reshape(-1, arrived.shape[-1])
    hidden = (
        jax.nn.silu(jnp.dot(flat_rows, gate_w, preferred_element_type=jnp.float32))
        * jnp.dot(flat_rows, up_w, preferred_element_type=jnp.float32)
    ).astype(jnp.bfloat16)
    return (
        jnp.dot(hidden, down_w, preferred_element_type=jnp.float32)
        .astype(jnp.bfloat16)
        .reshape(arrived.shape)
    )


def combine_rows(returned, slot_place, weights):
    picked = returned.reshape(-1, returned.shape[-1])[slot_place].reshape(
        weights.shape + (returned.shape[-1],)
    )
    return jnp.sum(weights[:, :, None] * picked.astype(jnp.float32), axis=1)


def shards(
    queries,
    keys,
    values,
    doc_ids,
    sink_logit,
    w_out,
    residual,
    ffn_gain,
    expert_ids,
    expert_weight,
    exp_gate,
    exp_up,
    exp_down,
    shared_gate,
    shared_up,
    shared_down,
):
    marks = (doc_ids + 1).astype(jnp.bfloat16)
    ext_keys, ext_values, ext_marks = (
        extended(keys, (("sp", 0),), WINDOW),
        extended(values, (("sp", 0),), WINDOW),
        extended(marks, (("sp", 0),), WINDOW),
    )
    attended = attend(queries, ext_keys, ext_values, ext_marks, marks, sink_logit)
    row_count = residual.shape[0]
    mixed = lax.psum_scatter(
        jnp.dot(attended, w_out, preferred_element_type=jnp.float32).astype(jnp.bfloat16),
        "tp",
        scatter_dimension=0,
        tiled=True,
    ).astype(jnp.float32)
    resid = (residual.astype(jnp.float32) + mixed).astype(jnp.bfloat16)
    resid_f = resid.astype(jnp.float32)
    normed = (
        resid_f
        * lax.rsqrt(jnp.mean(resid_f * resid_f, axis=-1, keepdims=True) + norm_eps)
        * ffn_gain
    ).astype(jnp.bfloat16)
    shard_rows = lax.all_gather(normed, "tp", axis=0, tiled=True)
    hidden = (
        jax.nn.silu(jnp.dot(shard_rows, shared_gate, preferred_element_type=jnp.float32))
        * jnp.dot(shard_rows, shared_up, preferred_element_type=jnp.float32)
    ).astype(jnp.bfloat16)
    partial_out = jnp.dot(hidden, shared_down, preferred_element_type=jnp.float32)
    shared_terms = lax.optimization_barrier(partial_out.astype(jnp.bfloat16)).astype(jnp.float32)
    shared_out = lax.psum_scatter(
        shared_terms.astype(jnp.bfloat16), "tp", scatter_dimension=0, tiled=True
    ).astype(jnp.float32)
    expert_count = lax.axis_size("sp") * exp_gate.shape[0]
    top_count = expert_ids.shape[1]
    half_rows = row_count // 2
    slot_cap = min(half_rows, max(2, 3 * half_rows * top_count // (2 * expert_count)))
    halves_out = []
    for half_index in range(2):
        first_row = half_index * half_rows
        part_ids = expert_ids[first_row : first_row + half_rows]
        part_rows = normed[first_row : first_row + half_rows]
        part_weight = expert_weight[first_row : first_row + half_rows]
        slot_place = slot_index(part_ids, half_rows, slot_cap, expert_count)
        packed = pack_rows(part_rows, slot_place, expert_count, slot_cap)
        returned = lax.all_to_all(
            run_expert(
                lax.all_to_all(packed, "sp", split_axis=0, concat_axis=0, tiled=True),
                exp_gate[0],
                exp_up[0],
                exp_down[0],
            ),
            "sp",
            split_axis=0,
            concat_axis=0,
            tiled=True,
        )
        halves_out.append(combine_rows(returned, slot_place, part_weight))
    routed = jnp.concatenate(halves_out, axis=0)
    return (resid.astype(jnp.float32) + shared_out + routed).astype(jnp.bfloat16)


def solution(mesh):
    placed = (
        P("sp", "tp"),
        P("sp", "tp"),
        P("sp", "tp"),
        P("sp"),
        P("tp"),
        P("tp", None),
        P(("sp", "tp"), None),
        P(),
        P(("sp", "tp"), None),
        P(("sp", "tp"), None),
        P("sp", None, None),
        P("sp", None, None),
        P("sp", None, None),
        P(None, "tp"),
        P(None, "tp"),
        P("tp", None),
    )
    return jax.shard_map(
        shards, mesh=mesh, in_specs=placed, out_specs=P(("sp", "tp"), None), check_vma=False
    )
```

profile of v0, /device:TPU:13, one launch (start us, length us, event | category | flops | bytes accessed | tf_op | source)
XLA Modules:
  0.0 713.2 jit_solution(18196577709892937796)
XLA Ops:
  7.4 3.7 collective-permute-start.2
  11.1 1.9 collective-permute-start.3
  13.0 1.4 fusion.52
  14.4 4.5 collective-permute-start.4
  19.0 1.9 collective-permute-start.5
  20.9 1.4 fusion.53
  22.3 4.5 collective-permute-start
  27.0 2.2 reshape.508
  29.9 1.9 collective-permute-start.1
  34.8 1.6 copy.65
  36.4 1.6 copy.66
  39.7 1.8 fusion.3
  41.5 1.8 fusion.2
  43.3 1.4 copy-done.1
  46.2 5.8 fusion.21
  52.7 2.6 convolution_convert_fusion.3
  55.6 4.5 reduce-window.14
  60.8 4.8 scatter_custom_fusion
  65.7 22.6 %reduce-scatter.3.cloned.1.call-done = bf16[256,2048]{1,0:T(8,128)(2,1)} async-done(((bf16[512,2048]{1,0:T(8,128)(2,1)}), bf16[256,2048]{1,0:T(8,128)(2,1)}) %reduce-scatter.3.cloned.1.call-update) | async-done | bytes 1048592 | tf_op jit(solution)/shard_map/reduce_scatter | solution.py:151
  88.2 1.6 fusion.7
  89.9 2.6 fusion.9
  92.5 1.3 fusion.49
  93.8 7.1 %gather_fusion.2 = bf16[1536,2048]{1,0:T(8,128)(2,1)} fusion(bf16[128,2048]{1,0:T(8,128)(2,1)S(1)} %get-tuple-element.6, s32[2048]{0:T(1024)S(1)} %pad_clamp_fusion.1), kind=kCustom, calls=%fused_computation.clone | custom fusion | bytes 12589056 | tf_op jit(solution)/shard_map/jit(_take)/gather | solution.py:101
  100.9 5.9 broadcast_select_fusion.1
  106.8 6.5 all-to-all-start
  113.5 4.5 reduce-window.16
  118.7 4.3 scatter_custom_fusion.1
  123.1 7.1 gather_fusion.3
  130.2 5.9 broadcast_select_fusion
  136.2 114.5 %all-to-all-done = bf16[16,96,2048]{2,1,0:T(8,128)(2,1)} async-done(((bf16[16,96,2048]{2,1,0:T(8,128)(2,1)}), bf16[16,96,2048]{2,1,0:T(8,128)(2,1)}, u32[]{:S(2)}, u32[]{:S(2)}) %all-to-all-start) | async-done | bytes 6291488 | tf_op jit(solution)/shard_map/all_to_all | solution.py:188
  250.7 4.8 all-to-all-start.2
  255.5 8.6 %fusion.18 = f32[1536,512]{1,0:T(8,128)} fusion(bf16[1536,2048]{1,0:T(8,128)(2,1)} %bitcast.18, bf16[1,2048,512]{2,1,0:T(8,128)(2,1)} %param.28), kind=kOutput, calls=%fused_computation.40 | convolution fusion | flops 3221225472 | bytes 11534336 | tf_op jit(solution)/shard_map/dot_general | solution.py:108
  264.1 11.7 %convolution_convert_fusion.1 = bf16[1536,2048]{1,0:T(8,128)(2,1)} fusion(bf16[1,512,2048]{2,1,0:T(8,128)(2,1)S(1)} %copy-done, bf16[1536,2048]{1,0:T(8,128)(2,1)} %bitcast.18, f32[1536,512]{1,0:T(8,128)} %fusion.18, bf16[1,2048,512]{2,1,0:T(8,128)(2,1)} %param.29), kind=kOutput, calls=%fused_computation.14 | convolution fusion | flops 6450315264 | bytes 19922944 | tf_op jit(solution)/shard_map/dot_general | solution.py:112
  275.8 117.1 %all-to-all-done.2 = bf16[16,96,2048]{2,1,0:T(8,128)(2,1)} async-done(((bf16[16,96,2048]{2,1,0:T(8,128)(2,1)}), bf16[16,96,2048]{2,1,0:T(8,128)(2,1)}, u32[]{:S(2)}, u32[]{:S(2)}) %all-to-all-start.2) | async-done | bytes 6291488 | tf_op jit(solution)/shard_map/all_to_all | solution.py:188
  392.9 5.1 all-to-all-start.1
  398.0 8.6 %fusion.16 = f32[1536,512]{1,0:T(8,128)} fusion(bf16[1536,2048]{1,0:T(8,128)(2,1)} %bitcast.32, bf16[1,2048,512]{2,1,0:T(8,128)(2,1)} %param.28), kind=kOutput, calls=%fused_computation.38 | convolution fusion | flops 3221225472 | bytes 11534336 | tf_op jit(solution)/shard_map/dot_general | solution.py:108
  406.6 11.7 %convolution_convert_fusion = bf16[1536,2048]{1,0:T(8,128)(2,1)} fusion(bf16[1,512,2048]{2,1,0:T(8,128)(2,1)S(1)} %copy-done, bf16[1536,2048]{1,0:T(8,128)(2,1)} %bitcast.32, f32[1536,512]{1,0:T(8,128)} %fusion.16, bf16[1,2048,512]{2,1,0:T(8,128)(2,1)} %param.29), kind=kOutput, calls=%fused_computation.13 | convolution fusion | flops 6450315264 | bytes 19922944 | tf_op jit(solution)/shard_map/dot_general | solution.py:112
  418.3 117.0 %all-to-all-done.1 = bf16[16,96,2048]{2,1,0:T(8,128)(2,1)} async-done(((bf16[16,96,2048]{2,1,0:T(8,128)(2,1)}), bf16[16,96,2048]{2,1,0:T(8,128)(2,1)}, u32[]{:S(2)}, u32[]{:S(2)}) %all-to-all-start.1) | async-done | bytes 6291488 | tf_op jit(solution)/shard_map/all_to_all | solution.py:186
  535.2 4.8 all-to-all-start.3
  540.8 34.2 %all-gather.2.cloned.1.call-done = bf16[512,2048]{1,0:T(8,128)(2,1)} async-done(((bf16[256,2048]{1,0:T(8,128)(2,1)}), bf16[512,2048]{1,0:T(8,128)(2,1)}) %all-gather.2.cloned.1.call-update) | async-done | bytes 2097168 | tf_op jit(solution)/shard_map/all_gather | solution.py:164
  575.0 2.6 fusion.57
  577.6 5.8 convolution_convert_fusion.2
  583.7 12.6 %gather_fusion = bf16[1024,2048]{1,0:T(8,128)(2,1)} fusion(bf16[1536,2048]{1,0:T(8,128)(2,1)} %bitcast.23, s32[1024]{0:T(1024)S(1)} %broadcast_clamp_fusion.1), kind=kCustom, calls=%fused_computation.2 | custom fusion | bytes 8392704 | tf_op jit(solution)/shard_map/gather | solution.py:119
  596.3 81.1 %all-to-all-done.3 = bf16[16,96,2048]{2,1,0:T(8,128)(2,1)} async-done(((bf16[16,96,2048]{2,1,0:T(8,128)(2,1)}), bf16[16,96,2048]{2,1,0:T(8,128)(2,1)}, u32[]{:S(2)}, u32[]{:S(2)}) %all-to-all-start.3) | async-done | bytes 6291488 | tf_op jit(solution)/shard_map/all_to_all | solution.py:186
  677.4 12.4 %gather_fusion.1 = bf16[1024,2048]{1,0:T(8,128)(2,1)} fusion(bf16[1536,2048]{1,0:T(8,128)(2,1)} %bitcast.34, s32[1024]{0:T(1024)S(1)} %broadcast_clamp_fusion), kind=kCustom, calls=%fused_computation.3 | custom fusion | bytes 8392704 | tf_op jit(solution)/shard_map/gather | solution.py:119
  689.8 7.6 %fusion.1 = f32[128,2048]{1,0:T(8,128)} fusion(bf16[1024,2048]{1,0:T(8,128)(2,1)} %gather_fusion, f32[128,8]{1,0:T(8,128)S(1)} %copy.45), kind=kLoop, calls=%fused_computation.9 | loop fusion | flops 6029312 | bytes 5246976 | tf_op jit(solution)/shard_map/reduce_sum | solution.py:122
  697.4 5.3 fusion
  702.7 3.7 fusion.11
  (108 shorter events, 11.4 us)
Async XLA Ops:
  6.5 257.5 %copy-start = (bf16[1,512,2048]{2,1,0:T(8,128)(2,1)S(1)}, bf16[1,512,2048]{2,1,0:T(8,128)(2,1)}, u32[]{:S(2)}) copy-start(bf16[1,512,2048]{2,1,0:T(8,128)(2,1)} %param.30) | copy-start | bytes 6291460
  6.5 81.7 %reduce-scatter.3.cloned.1.call-start = ((), (), s32[]{:S(2)}) async-start(), calls=%async_computation.6 | async-start | bytes 3145728 | tf_op jit(solution)/shard_map/reduce_scatter | solution.py:151
  7.4 22.5 %collective-permute-start.2 = (bf16[128]{0:T(256)(128)(2,1)S(1)}, bf16[128]{0:T(256)(128)(2,1)S(1)}, u32[]{:S(2)}, u32[]{:S(2)}) collective-permute-start(bf16[128]{0:T(256)(128)(2,1)S(1)} %get-tuple-element.26), channel_id=1, source_target_pairs={{0,2},{2,4},{4,6},{6,8},{8,10},{10,12},{12,14},{14,16},{16,18},{18... | collective-permute-start | bytes 776 | tf_op jit(solution)/shard_map/ppermute | solution.py:19
  11.1 20.8 %collective-permute-start.3 = (bf16[128]{0:T(256)(128)(2,1)S(1)}, bf16[128]{0:T(256)(128)(2,1)S(1)}, u32[]{:S(2)}, u32[]{:S(2)}) collective-permute-start(bf16[128]{0:T(256)(128)(2,1)S(1)} %get-tuple-element.27), channel_id=1, source_target_pairs={{2,0},{4,2},{6,4},{8,6},{10,8},{12,10},{14,12},{16,14},{18,16},{20... | collective-permute-start | bytes 776 | tf_op jit(solution)/shard_map/ppermute | solution.py:21
  14.4 17.8 %collective-permute-start.4 = (bf16[128,128]{1,0:T(8,128)(2,1)}, bf16[128,128]{1,0:T(8,128)(2,1)}, u32[]{:S(2)}, u32[]{:S(2)}) collective-permute-start(bf16[128,128]{1,0:T(8,128)(2,1)} %get-tuple-element.16), channel_id=1, source_target_pairs={{0,2},{2,4},{4,6},{6,8},{8,10},{10,12},{12,14},{14,16},{16,18},{18... | collective-permute-start | bytes 98312 | tf_op jit(solution)/shard_map/ppermute | solution.py:19
  19.0 13.3 %collective-permute-start.5 = (bf16[128,128]{1,0:T(8,128)(2,1)}, bf16[128,128]{1,0:T(8,128)(2,1)}, u32[]{:S(2)}, u32[]{:S(2)}) collective-permute-start(bf16[128,128]{1,0:T(8,128)(2,1)} %get-tuple-element.17), channel_id=1, source_target_pairs={{2,0},{4,2},{6,4},{8,6},{10,8},{12,10},{14,12},{16,14},{18,16},{20... | collective-permute-start | bytes 98312 | tf_op jit(solution)/shard_map/ppermute | solution.py:21
  22.3 22.5 %collective-permute-start = (bf16[128,128]{1,0:T(8,128)(2,1)}, bf16[128,128]{1,0:T(8,128)(2,1)}, u32[]{:S(2)}, u32[]{:S(2)}) collective-permute-start(bf16[128,128]{1,0:T(8,128)(2,1)} %get-tuple-element.18), channel_id=1, source_target_pairs={{0,2},{2,4},{4,6},{6,8},{8,10},{10,12},{12,14},{14,16},{16,18},{18... | collective-permute-start | bytes 98312 | tf_op jit(solution)/shard_map/ppermute | solution.py:19
  29.9 14.8 %collective-permute-start.1 = (bf16[128,128]{1,0:T(8,128)(2,1)}, bf16[128,128]{1,0:T(8,128)(2,1)}, u32[]{:S(2)}, u32[]{:S(2)}) collective-permute-start(bf16[128,128]{1,0:T(8,128)(2,1)} %get-tuple-element.19), channel_id=1, source_target_pairs={{2,0},{4,2},{6,4},{8,6},{10,8},{12,10},{14,12},{16,14},{18,16},{20... | collective-permute-start | bytes 98312 | tf_op jit(solution)/shard_map/ppermute | solution.py:21
  41.4 3.2 copy-start.1
  41.5 3.2 copy-start.5
  46.2 6.5 copy-start.9
  52.7 2.7 copy-start.7
  55.3 32.9 %copy-start.3 = (bf16[256,2048]{1,0:T(8,128)(2,1)S(1)}, bf16[256,2048]{1,0:T(8,128)(2,1)}, u32[]{:S(2)}) copy-start(bf16[256,2048]{1,0:T(8,128)(2,1)} %param.24) | copy-start | bytes 3145732
  55.3 34.6 %copy-start.6 = (f32[2048]{0:T(1024)S(1)}, f32[2048]{0:T(1024)}, u32[]{:S(2)}) copy-start(f32[2048]{0:T(1024)} %param.25) | copy-start | bytes 24580
  106.8 143.9 %all-to-all-start = ((bf16[16,96,2048]{2,1,0:T(8,128)(2,1)}), bf16[16,96,2048]{2,1,0:T(8,128)(2,1)}, u32[]{:S(2)}, u32[]{:S(2)}) async-start(bf16[16,96,2048]{2,1,0:T(8,128)(2,1)} %bitcast.114), calls=%async_computation.2 | async-start | bytes 12582912 | tf_op jit(solution)/shard_map/all_to_all | solution.py:188
  250.7 142.2 %all-to-all-start.2 = ((bf16[16,96,2048]{2,1,0:T(8,128)(2,1)}), bf16[16,96,2048]{2,1,0:T(8,128)(2,1)}, u32[]{:S(2)}, u32[]{:S(2)}) async-start(bf16[16,96,2048]{2,1,0:T(8,128)(2,1)} %bitcast.115), calls=%async_computation.4 | async-start | bytes 12582912 | tf_op jit(solution)/shard_map/all_to_all | solution.py:188
  392.9 142.4 %all-to-all-start.1 = ((bf16[16,96,2048]{2,1,0:T(8,128)(2,1)}), bf16[16,96,2048]{2,1,0:T(8,128)(2,1)}, u32[]{:S(2)}, u32[]{:S(2)}) async-start(bf16[16,96,2048]{2,1,0:T(8,128)(2,1)} %bitcast.117), calls=%async_computation.3 | async-start | bytes 12582912 | tf_op jit(solution)/shard_map/all_to_all | solution.py:186
  535.2 142.2 %all-to-all-start.3 = ((bf16[16,96,2048]{2,1,0:T(8,128)(2,1)}), bf16[16,96,2048]{2,1,0:T(8,128)(2,1)}, u32[]{:S(2)}, u32[]{:S(2)}) async-start(bf16[16,96,2048]{2,1,0:T(8,128)(2,1)} %bitcast.116), calls=%async_computation.5 | async-start | bytes 12582912 | tf_op jit(solution)/shard_map/all_to_all | solution.py:186
  540.0 35.0 %all-gather.2.cloned.1.call-start = ((), (), s32[]{:S(2)}) async-start(), calls=%async_computation.7 | async-start | bytes 3145728 | tf_op jit(solution)/shard_map/all_gather | solution.py:164
  540.7 162.0 %reduce-scatter.5.cloned.1.call-start = ((), (), s32[]{:S(2)}) async-start(), calls=%async_computation.8 | async-start | bytes 3145728 | tf_op jit(solution)/shard_map/reduce_scatter | solution.py:171
  577.6 5.9 copy-start.8
  689.8 7.6 %copy-start.2 = (bf16[1024,2048]{1,0:T(8,128)(2,1)S(1)}, bf16[1024,2048]{1,0:T(8,128)(2,1)}, u32[]{:S(2)}) copy-start(bf16[1024,2048]{1,0:T(8,128)(2,1)} %gather_fusion.1) | copy-start | bytes 12582916
  697.4 5.3 copy-start.4
Sparse Core Ops, SparseCore 0:
  55.4 32.7 reduce-scatter.2
  542.4 32.5 all-gather.1
  583.5 31.8 reduce-scatter.4
where the time goes:
time: 722 us; the launch traced here: 713 us
  waiting for transfers between devices  487 us (67%)
  local copies, waits for them, and re-layouts  65.4 us (9%)
  matrix products  59.3 us (8%)
  other arithmetic  47.8 us (7%)
  starting transfers between devices  39.7 us (5%)
  between operations  13.8 us (2%)
    all_to_all x2, waiting for transfers between devices, shards(): lax.all_to_all(packed, 'sp', split_axis=0, concat_axis=0, tiled=True)  232 us
    all_to_all x2, waiting for transfers between devices, shards(): lax.all_to_all(run_expert(lax.all_to_all(packed, 'sp', split_axis=0, conc...  198 us
    all_gather x1, waiting for transfers between devices, shards(): shard_rows = lax.all_gather(normed, 'tp', axis=0, tiled=True)  34.2 us
    gather x2, local copies, waits for them, and re-layouts, combine_rows(): returned.reshape(-1, returned.shape[-1])[slot_place]  25.1 us
    dot_general x2, matrix products, run_expert(): jnp.dot(hidden, down_w, preferred_element_type=jnp.float32)  23.4 us
    reduce_scatter x1, waiting for transfers between devices, shards(): lax.psum_scatter(jnp.dot(attended, w_out, preferred_element_type=jnp.floa...  22.6 us
    dot_general x2, matrix products, run_expert(): jnp.dot(flat_rows, gate_w, preferred_element_type=jnp.float32)  17.2 us
  transfers between devices with their start and end apart: 13, of which 6 were waited for; matrix products, arithmetic and copies ran while one was open for 19% of the time, Pallas kernels for 0%

commit v1 on v0

--- a/solution.py
+++ b/solution.py
@@ -161,7 +161,9 @@
         * lax.rsqrt(jnp.mean(resid_f * resid_f, axis=-1, keepdims=True) + norm_eps)
         * ffn_gain
     ).astype(jnp.bfloat16)
-    shard_rows = lax.all_gather(normed, "tp", axis=0, tiled=True)
+    shard_rows = jnp.concatenate(
+        lax.all_to_all(jnp.stack([normed] * lax.axis_size("tp")), "tp", 0, 0), axis=0
+    )
     hidden = (
         jax.nn.silu(jnp.dot(shard_rows, shared_gate, preferred_element_type=jnp.float32))
         * jnp.dot(shard_rows, shared_up, preferred_element_type=jnp.float32)

time: 722 us -> 739 us (1.024)
  waiting for transfers between devices: 487 us -> 498 us
    all_to_all x2, waiting for transfers between devices: 198 us -> 233 us  [shards(): lax.all_to_all(run_expert(lax.all_to_all(packed, 'sp', split_axis=0, conc...]
    all_gather x1 -> x0, waiting for transfers between devices: 34.2 us -> none  [shards(): shard_rows = lax.all_gather(normed, 'tp', axis=0, tiled=True)]
    all_to_all x0 -> x1, waiting for transfers between devices: none -> 11.1 us  [shards(): lax.all_to_all(jnp.stack([normed] * lax.axis_size('tp')), 'tp', 0, 0)]
  transfers between devices with their start and end apart: 13 -> 13, of which waited for: 6 -> 6; matrix products, arithmetic and copies ran while one was open for 19% -> 21% of each run, Pallas kernels for 0% -> 0%
where the time goes in v1:
time: 739 us; the launch traced here: 730 us
  waiting for transfers between devices  498 us (67%)
  local copies, waits for them, and re-layouts  64.3 us (9%)
  matrix products  59.4 us (8%)
  other arithmetic  48.4 us (7%)
  starting transfers between devices  45.3 us (6%)
  between operations  14.2 us (2%)
    all_to_all x2, waiting for transfers between devices, shards(): lax.all_to_all(run_expert(lax.all_to_all(packed, 'sp', split_axis=0, conc...  233 us
    all_to_all x2, waiting for transfers between devices, shards(): lax.all_to_all(packed, 'sp', split_axis=0, concat_axis=0, tiled=True)  232 us
    gather x2, local copies, waits for them, and re-layouts, combine_rows(): returned.reshape(-1, returned.shape[-1])[slot_place]  25.1 us
    dot_general x2, matrix products, run_expert(): jnp.dot(hidden, down_w, preferred_element_type=jnp.float32)  23.5 us
    reduce_scatter x1, waiting for transfers between devices, shards(): lax.psum_scatter(jnp.dot(attended, w_out, preferred_element_type=jnp.floa...  22.6 us
    dot_general x2, matrix products, run_expert(): jnp.dot(flat_rows, gate_w, preferred_element_type=jnp.float32)  17.2 us
  transfers between devices with their start and end apart: 13, of which 6 were waited for; matrix products, arithmetic and copies ran while one was open for 21% of the time, Pallas kernels for 0%

profile of v1, /device:TPU:13, one launch (start us, length us, event | category | flops | bytes accessed | tf_op | source)
XLA Modules:
  0.0 729.7 jit_solution(13917517417858374231)
XLA Ops:
  7.4 3.7 collective-permute-start.2
  11.1 1.9 collective-permute-start.3
  13.0 1.4 fusion.52
  14.4 4.5 collective-permute-start.4
  19.0 1.9 collective-permute-start.5
  20.9 1.4 fusion.53
  22.3 4.5 collective-permute-start
  27.0 2.2 reshape.512
  29.9 1.9 collective-permute-start.1
  34.8 1.6 copy.65
  36.4 1.6 copy.66
  39.7 1.8 fusion.3
  41.5 1.8 fusion.2
  46.2 5.8 fusion.21
  52.7 2.6 convolution_convert_fusion.3
  55.6 4.5 reduce-window.14
  60.8 4.8 scatter_custom_fusion
  65.7 22.6 %reduce-scatter.3.cloned.1.call-done = bf16[256,2048]{1,0:T(8,128)(2,1)} async-done(((bf16[512,2048]{1,0:T(8,128)(2,1)}), bf16[256,2048]{1,0:T(8,128)(2,1)}) %reduce-scatter.3.cloned.1.call-update) | async-done | bytes 1048592 | tf_op jit(solution)/shard_map/reduce_scatter | solution.py:151
  88.2 1.6 fusion.7
  89.9 1.7 fusion.9
  91.7 1.5 pad_maximum_fusion
  93.2 4.8 all-to-all-start
  98.0 7.1 gather_fusion.2
  105.1 5.9 broadcast_select_fusion.1
  111.0 11.1 %all-to-all-done = bf16[2,256,2048]{2,1,0:T(8,128)(2,1)} async-done(((bf16[2,256,2048]{2,1,0:T(8,128)(2,1)}), bf16[2,256,2048]{2,1,0:T(8,128)(2,1)}, u32[]{:S(2)}, u32[]{:S(2)}) %all-to-all-start) | async-done | bytes 2097184 | tf_op jit(solution)/shard_map/all_to_all | solution.py:165
  122.1 7.3 %all-to-all-start.1 = ((bf16[16,96,2048]{2,1,0:T(8,128)(2,1)}), bf16[16,96,2048]{2,1,0:T(8,128)(2,1)}, u32[]{:S(2)}, u32[]{:S(2)}) async-start(bf16[16,96,2048]{2,1,0:T(8,128)(2,1)} %bitcast.116), calls=%async_computation.3 | async-start | bytes 12582912 | tf_op jit(solution)/shard_map/all_to_all | solution.py:190
  129.7 4.5 reduce-window.16
  134.9 4.3 scatter_custom_fusion.1
  139.3 7.1 gather_fusion.3
  146.4 5.9 broadcast_select_fusion
  152.3 114.5 %all-to-all-done.1 = bf16[16,96,2048]{2,1,0:T(8,128)(2,1)} async-done(((bf16[16,96,2048]{2,1,0:T(8,128)(2,1)}), bf16[16,96,2048]{2,1,0:T(8,128)(2,1)}, u32[]{:S(2)}, u32[]{:S(2)}) %all-to-all-start.1) | async-done | bytes 6291488 | tf_op jit(solution)/shard_map/all_to_all | solution.py:190
  266.9 4.8 all-to-all-start.3
  271.7 8.6 %fusion.18 = f32[1536,512]{1,0:T(8,128)} fusion(bf16[1536,2048]{1,0:T(8,128)(2,1)} %bitcast.20, bf16[1,2048,512]{2,1,0:T(8,128)(2,1)} %param.28), kind=kOutput, calls=%fused_computation.41 | convolution fusion | flops 3221225472 | bytes 11534336 | tf_op jit(solution)/shard_map/dot_general | solution.py:108
  280.3 11.8 %convolution_convert_fusion.1 = bf16[1536,2048]{1,0:T(8,128)(2,1)} fusion(bf16[1,512,2048]{2,1,0:T(8,128)(2,1)S(1)} %copy-done, bf16[1536,2048]{1,0:T(8,128)(2,1)} %bitcast.20, f32[1536,512]{1,0:T(8,128)} %fusion.18, bf16[1,2048,512]{2,1,0:T(8,128)(2,1)} %param.29), kind=kOutput, calls=%fused_computation.14 | convolution fusion | flops 6450315264 | bytes 19922944 | tf_op jit(solution)/shard_map/dot_general | solution.py:112
  292.0 117.0 %all-to-all-done.3 = bf16[16,96,2048]{2,1,0:T(8,128)(2,1)} async-done(((bf16[16,96,2048]{2,1,0:T(8,128)(2,1)}), bf16[16,96,2048]{2,1,0:T(8,128)(2,1)}, u32[]{:S(2)}, u32[]{:S(2)}) %all-to-all-start.3) | async-done | bytes 6291488 | tf_op jit(solution)/shard_map/all_to_all | solution.py:190
  409.1 5.1 all-to-all-start.2
  414.2 8.6 %fusion.16 = f32[1536,512]{1,0:T(8,128)} fusion(bf16[1536,2048]{1,0:T(8,128)(2,1)} %bitcast.34, bf16[1,2048,512]{2,1,0:T(8,128)(2,1)} %param.28), kind=kOutput, calls=%fused_computation.39 | convolution fusion | flops 3221225472 | bytes 11534336 | tf_op jit(solution)/shard_map/dot_general | solution.py:108
  422.8 11.7 %convolution_convert_fusion = bf16[1536,2048]{1,0:T(8,128)(2,1)} fusion(bf16[1,512,2048]{2,1,0:T(8,128)(2,1)S(1)} %copy-done, bf16[1536,2048]{1,0:T(8,128)(2,1)} %bitcast.34, f32[1536,512]{1,0:T(8,128)} %fusion.16, bf16[1,2048,512]{2,1,0:T(8,128)(2,1)} %param.29), kind=kOutput, calls=%fused_computation.13 | convolution fusion | flops 6450315264 | bytes 19922944 | tf_op jit(solution)/shard_map/dot_general | solution.py:112
  434.5 116.9 %all-to-all-done.2 = bf16[16,96,2048]{2,1,0:T(8,128)(2,1)} async-done(((bf16[16,96,2048]{2,1,0:T(8,128)(2,1)}), bf16[16,96,2048]{2,1,0:T(8,128)(2,1)}, u32[]{:S(2)}, u32[]{:S(2)}) %all-to-all-start.2) | async-done | bytes 6291488 | tf_op jit(solution)/shard_map/all_to_all | solution.py:188
  551.4 4.8 all-to-all-start.4
  556.2 2.6 fusion.57
  558.8 5.8 convolution_convert_fusion.2
  564.9 12.6 %gather_fusion = bf16[1024,2048]{1,0:T(8,128)(2,1)} fusion(bf16[1536,2048]{1,0:T(8,128)(2,1)} %bitcast.25, s32[1024]{0:T(1024)S(1)} %broadcast_clamp_fusion.1), kind=kCustom, calls=%fused_computation.2 | custom fusion | bytes 8392704 | tf_op jit(solution)/shard_map/gather | solution.py:119
  577.6 116.0 %all-to-all-done.4 = bf16[16,96,2048]{2,1,0:T(8,128)(2,1)} async-done(((bf16[16,96,2048]{2,1,0:T(8,128)(2,1)}), bf16[16,96,2048]{2,1,0:T(8,128)(2,1)}, u32[]{:S(2)}, u32[]{:S(2)}) %all-to-all-start.4) | async-done | bytes 6291488 | tf_op jit(solution)/shard_map/all_to_all | solution.py:188
  693.6 12.4 %gather_fusion.1 = bf16[1024,2048]{1,0:T(8,128)(2,1)} fusion(bf16[1536,2048]{1,0:T(8,128)(2,1)} %bitcast.36, s32[1024]{0:T(1024)S(1)} %broadcast_clamp_fusion), kind=kCustom, calls=%fused_computation.3 | custom fusion | bytes 8392704 | tf_op jit(solution)/shard_map/gather | solution.py:119
  706.0 7.6 %fusion.1 = f32[128,2048]{1,0:T(8,128)} fusion(bf16[1024,2048]{1,0:T(8,128)(2,1)} %gather_fusion, f32[128,8]{1,0:T(8,128)S(1)} %copy.45), kind=kLoop, calls=%fused_computation.9 | loop fusion | flops 6029312 | bytes 5246976 | tf_op jit(solution)/shard_map/reduce_sum | solution.py:122
  713.6 5.3 fusion
  718.9 3.7 fusion.11
  (108 shorter events, 12.1 us)
Async XLA Ops:
  6.5 273.7 %copy-start = (bf16[1,512,2048]{2,1,0:T(8,128)(2,1)S(1)}, bf16[1,512,2048]{2,1,0:T(8,128)(2,1)}, u32[]{:S(2)}) copy-start(bf16[1,512,2048]{2,1,0:T(8,128)(2,1)} %param.30) | copy-start | bytes 6291460
  6.5 81.7 %reduce-scatter.3.cloned.1.call-start = ((), (), s32[]{:S(2)}) async-start(), calls=%async_computation.7 | async-start | bytes 3145728 | tf_op jit(solution)/shard_map/reduce_scatter | solution.py:151
  7.4 22.5 %collective-permute-start.2 = (bf16[128]{0:T(256)(128)(2,1)S(1)}, bf16[128]{0:T(256)(128)(2,1)S(1)}, u32[]{:S(2)}, u32[]{:S(2)}) collective-permute-start(bf16[128]{0:T(256)(128)(2,1)S(1)} %get-tuple-element.26), channel_id=1, source_target_pairs={{0,2},{2,4},{4,6},{6,8},{8,10},{10,12},{12,14},{14,16},{16,18},{18... | collective-permute-start | bytes 776 | tf_op jit(solution)/shard_map/ppermute | solution.py:19
  11.1 20.8 %collective-permute-start.3 = (bf16[128]{0:T(256)(128)(2,1)S(1)}, bf16[128]{0:T(256)(128)(2,1)S(1)}, u32[]{:S(2)}, u32[]{:S(2)}) collective-permute-start(bf16[128]{0:T(256)(128)(2,1)S(1)} %get-tuple-element.27), channel_id=1, source_target_pairs={{2,0},{4,2},{6,4},{8,6},{10,8},{12,10},{14,12},{16,14},{18,16},{20... | collective-permute-start | bytes 776 | tf_op jit(solution)/shard_map/ppermute | solution.py:21
  14.4 17.8 %collective-permute-start.4 = (bf16[128,128]{1,0:T(8,128)(2,1)}, bf16[128,128]{1,0:T(8,128)(2,1)}, u32[]{:S(2)}, u32[]{:S(2)}) collective-permute-start(bf16[128,128]{1,0:T(8,128)(2,1)} %get-tuple-element.16), channel_id=1, source_target_pairs={{0,2},{2,4},{4,6},{6,8},{8,10},{10,12},{12,14},{14,16},{16,18},{18... | collective-permute-start | bytes 98312 | tf_op jit(solution)/shard_map/ppermute | solution.py:19
  19.0 13.3 %collective-permute-start.5 = (bf16[128,128]{1,0:T(8,128)(2,1)}, bf16[128,128]{1,0:T(8,128)(2,1)}, u32[]{:S(2)}, u32[]{:S(2)}) collective-permute-start(bf16[128,128]{1,0:T(8,128)(2,1)} %get-tuple-element.17), channel_id=1, source_target_pairs={{2,0},{4,2},{6,4},{8,6},{10,8},{12,10},{14,12},{16,14},{18,16},{20... | collective-permute-start | bytes 98312 | tf_op jit(solution)/shard_map/ppermute | solution.py:21
  22.3 22.5 %collective-permute-start = (bf16[128,128]{1,0:T(8,128)(2,1)}, bf16[128,128]{1,0:T(8,128)(2,1)}, u32[]{:S(2)}, u32[]{:S(2)}) collective-permute-start(bf16[128,128]{1,0:T(8,128)(2,1)} %get-tuple-element.18), channel_id=1, source_target_pairs={{0,2},{2,4},{4,6},{6,8},{8,10},{10,12},{12,14},{14,16},{16,18},{18... | collective-permute-start | bytes 98312 | tf_op jit(solution)/shard_map/ppermute | solution.py:19
  29.9 14.8 %collective-permute-start.1 = (bf16[128,128]{1,0:T(8,128)(2,1)}, bf16[128,128]{1,0:T(8,128)(2,1)}, u32[]{:S(2)}, u32[]{:S(2)}) collective-permute-start(bf16[128,128]{1,0:T(8,128)(2,1)} %get-tuple-element.19), channel_id=1, source_target_pairs={{2,0},{4,2},{6,4},{8,6},{10,8},{12,10},{14,12},{16,14},{18,16},{20... | collective-permute-start | bytes 98312 | tf_op jit(solution)/shard_map/ppermute | solution.py:21
  41.4 3.2 copy-start.1
  41.5 3.2 copy-start.5
  46.2 6.5 copy-start.9
  52.7 2.7 copy-start.7
  55.3 32.9 %copy-start.3 = (bf16[256,2048]{1,0:T(8,128)(2,1)S(1)}, bf16[256,2048]{1,0:T(8,128)(2,1)}, u32[]{:S(2)}) copy-start(bf16[256,2048]{1,0:T(8,128)(2,1)} %param.24) | copy-start | bytes 3145732
  55.3 34.6 %copy-start.6 = (f32[2048]{0:T(1024)S(1)}, f32[2048]{0:T(1024)}, u32[]{:S(2)}) copy-start(f32[2048]{0:T(1024)} %param.25) | copy-start | bytes 24580
  93.2 29.0 %all-to-all-start = ((bf16[2,256,2048]{2,1,0:T(8,128)(2,1)}), bf16[2,256,2048]{2,1,0:T(8,128)(2,1)}, u32[]{:S(2)}, u32[]{:S(2)}) async-start(bf16[2,256,2048]{2,1,0:T(8,128)(2,1)} %pad_maximum_fusion), calls=%async_computation.1 | async-start | bytes 4194304 | tf_op jit(solution)/shard_map/all_to_all | solution.py:165
  122.1 144.7 %all-to-all-start.1 = ((bf16[16,96,2048]{2,1,0:T(8,128)(2,1)}), bf16[16,96,2048]{2,1,0:T(8,128)(2,1)}, u32[]{:S(2)}, u32[]{:S(2)}) async-start(bf16[16,96,2048]{2,1,0:T(8,128)(2,1)} %bitcast.116), calls=%async_computation.3 | async-start | bytes 12582912 | tf_op jit(solution)/shard_map/all_to_all | solution.py:190
  266.9 142.2 %all-to-all-start.3 = ((bf16[16,96,2048]{2,1,0:T(8,128)(2,1)}), bf16[16,96,2048]{2,1,0:T(8,128)(2,1)}, u32[]{:S(2)}, u32[]{:S(2)}) async-start(bf16[16,96,2048]{2,1,0:T(8,128)(2,1)} %bitcast.117), calls=%async_computation.5 | async-start | bytes 12582912 | tf_op jit(solution)/shard_map/all_to_all | solution.py:190
  409.1 142.4 %all-to-all-start.2 = ((bf16[16,96,2048]{2,1,0:T(8,128)(2,1)}), bf16[16,96,2048]{2,1,0:T(8,128)(2,1)}, u32[]{:S(2)}, u32[]{:S(2)}) async-start(bf16[16,96,2048]{2,1,0:T(8,128)(2,1)} %bitcast.120), calls=%async_computation.4 | async-start | bytes 12582912 | tf_op jit(solution)/shard_map/all_to_all | solution.py:188
  551.4 142.2 %all-to-all-start.4 = ((bf16[16,96,2048]{2,1,0:T(8,128)(2,1)}), bf16[16,96,2048]{2,1,0:T(8,128)(2,1)}, u32[]{:S(2)}, u32[]{:S(2)}) async-start(bf16[16,96,2048]{2,1,0:T(8,128)(2,1)} %bitcast.119), calls=%async_computation.6 | async-start | bytes 12582912 | tf_op jit(solution)/shard_map/all_to_all | solution.py:188
  556.2 162.7 %reduce-scatter.5.cloned.1.call-start = ((), (), s32[]{:S(2)}) async-start(), calls=%async_computation.8 | async-start | bytes 3145728 | tf_op jit(solution)/shard_map/reduce_scatter | solution.py:173
  558.8 5.9 copy-start.8
  706.0 7.6 %copy-start.2 = (bf16[1024,2048]{1,0:T(8,128)(2,1)S(1)}, bf16[1024,2048]{1,0:T(8,128)(2,1)}, u32[]{:S(2)}) copy-start(bf16[1024,2048]{1,0:T(8,128)(2,1)} %gather_fusion.1) | copy-start | bytes 12582916
  713.6 5.3 copy-start.4
Sparse Core Ops, SparseCore 0:
  55.4 32.7 reduce-scatter.2
  564.8 31.4 reduce-scatter.4
